TPU v7x, 32 devices: a whole 2x2x4 slice. The times are simulated.
32 devices in a mesh: grp: 2 (over y), sp: 4 (over z), tp: 4 (over x, core).
Axes of the slice: x: 2, y: 2, z: 4, core: 2. Of those that a mesh axis runs over, the one named last changes fastest.
Arguments:
- tokens: bfloat16 [256, 8, 2048], P(('sp', 'tp'), 'grp'), parts along dimension 1, may hold values from -6 to 6
- norm_gain: float32 [2048], replicated, may hold values from 0.1 to 1.9
- w_query: bfloat16 [2048, 2048], P('sp', 'tp'), may hold values from -0.125 to 0.125
- w_value: bfloat16 [2048, 2048], P('sp', 'tp'), may hold values from -0.125 to 0.125
- w_fwd_gate: bfloat16 [2048, 2048], P('sp', 'tp'), may hold values from -0.125 to 0.125
- w_bwd_gate: bfloat16 [2048, 2048], P('sp', 'tp'), may hold values from -0.125 to 0.125
- w_out_gate: bfloat16 [2048, 2048], P('sp', 'tp'), may hold values from -0.125 to 0.125
- floor_gap: float32 [2, 2048], P(None, 'tp'), may hold values from 0.00078125 to 0.1
- decay_shift: float32 [256, 8, 2048], P('sp', 'grp', 'tp'), parts along dimension 1, may hold values from -1.1 to 0
- head_gain: float32 [128], replicated, may hold values from 0.1 to 1.9
- w_out: bfloat16 [2048, 2048], P('tp', 'sp'), may hold values from -0.125 to 0.125
Outputs:
- layer_out: bfloat16 [256, 8, 2048], P(('sp', 'tp'), 'grp'), parts along dimension 1
There are 2 independent parts, one for each index of `grp`. A program takes and returns all parts, laid end to end along the dimension named above; an argument that names none is the same for every part. Nothing has to cross between parts.
All inputs are finite; a program needn't handle non-finite values.
Results may differ from a plain program's by a relative error of at most 0.013.
Values may be sent and summed in bfloat16 or wider, within the bound.
A program may use at most 128 MiB of HBM per device.

v0:
```python
import jax
import jax.numpy as jnp
from jax import lax
from jax.sharding import PartitionSpec as P

KEY = 128
VAL = 128
BLOCK = 64
norm_eps = 1e-06
highest = lax.Precision.HIGHEST


def carried_in(x, axis, join, neutral, backward):
    count = lax.axis_size(axis)
    place = lax.axis_index(axis)
    ahead = count - 1 - place if backward else place
    gathered = jax.tree.map(
        lambda a, kind: lax.all_gather(a.astype(kind), axis), x, (jnp.bfloat16, jnp.bfloat16)
    )
    state = jax.tree.map(lambda a, e: jnp.zeros_like(a) + jnp.asarray(e, a.dtype), x, neutral)

    def one(turn, state):
        source = count - 1 - turn if backward else turn
        return join(
            state,
            jax.tree.map(
                lambda a, own: lax.dynamic_index_in_dim(a, source, 0, False).astype(own.dtype),
                gathered,
                x,
            ),
        )

    return lax.fori_loop(0, ahead, one, state)


def split_blocks(array):
    return array.reshape(array.shape[0] // BLOCK, BLOCK, *array.shape[1:])


def prepare_chain(queries, key_cols, values, log_decay):
    query_blocks = split_blocks(queries)
    key_blocks = split_blocks(key_cols)
    value_blocks = split_blocks(values)
    running = jnp.cumsum(split_blocks(log_decay), axis=1)
    block_end = running[:, -1]
    block_state = jnp.einsum(
        "nsbhk,nsbhe->nbhke",
        key_blocks * jnp.exp(block_end[:, None] - running),
        value_blocks,
        precision=highest,
    )
    carry_state = jnp.zeros_like(block_state[0])
    log_total = jnp.zeros_like(block_end[0])
    offsets = [log_total]
    carry_state = jnp.exp(block_end[0])[..., None] * carry_state + block_state[0]
    log_total = block_end[0]
    return (
        query_blocks,
        key_blocks,
        value_blocks,
        running,
        block_state,
        jnp.stack(offsets),
        log_total,
        carry_state,
    )


def local_pass(chain, carry_state):
    query_blocks, key_blocks, value_blocks, running, block_state = (
        chain[0],
        chain[1],
        chain[2],
        chain[3],
        chain[4],
    )
    block_len = running.shape[1]
    earlier_mask = jnp.arange(block_len)[:, None] >= jnp.arange(block_len)[None, :]
    here = running[0]
    anchor = here[:1]
    query_scaled = query_blocks[0] * jnp.exp(here - anchor)
    key_scaled = key_blocks[0] * jnp.exp(anchor - here)
    scores = jnp.einsum("tbhk,sbhk->bhts", query_scaled, key_scaled, precision=highest)
    scores = jnp.where(earlier_mask, scores, 0.0)
    within = jnp.einsum("bhts,sbhe->tbhe", scores, value_blocks[0], precision=highest)
    carried = jnp.einsum(
        "tbhk,bhke->tbhe", query_blocks[0] * jnp.exp(here), carry_state, precision=highest
    )
    outputs = within + carried
    return outputs


def combine(earlier, later):
    return (earlier[0] + later[0], jnp.exp(later[0])[..., None] * earlier[1] + later[1])


def group_sums(flat_mixed, weight_lines, group_count):
    group_width = flat_mixed.shape[1] // group_count
    accumulated_total = jnp.zeros((flat_mixed.shape[0], weight_lines.shape[1]), jnp.float32)
    for tp_group in range(group_count):
        first_column = tp_group * group_width
        partial_value = jnp.dot(
            flat_mixed[:, first_column : first_column + group_width],
            weight_lines[first_column : first_column + group_width],
            preferred_element_type=jnp.float32,
        ).astype(jnp.bfloat16)
        accumulated_total = accumulated_total + lax.optimization_barrier(partial_value).astype(
            jnp.float32
        )
    return accumulated_total


def shards(
    tokens,
    norm_gain,
    w_query,
    w_value,
    w_fwd_gate,
    w_bwd_gate,
    w_out_gate,
    floor_gap,
    decay_shift,
    head_gain,
    w_out,
):
    token_f32 = tokens.astype(jnp.float32)
    scale_rows = lax.rsqrt(jnp.mean(token_f32 * token_f32, axis=-1, keepdims=True) + norm_eps)
    normed = (token_f32 * scale_rows * norm_gain).astype(jnp.bfloat16)
    weights = (
        lax.all_gather(w_query, "sp", axis=0, tiled=True),
        lax.all_gather(w_value, "sp", axis=0, tiled=True),
        lax.all_gather(w_fwd_gate, "sp", axis=0, tiled=True),
        lax.all_gather(w_bwd_gate, "sp", axis=0, tiled=True),
        lax.all_gather(w_out_gate, "sp", axis=0, tiled=True),
    )
    piece_rows = lax.all_gather(normed, "tp", axis=0, tiled=True)
    flat_rows = piece_rows.reshape(-1, piece_rows.shape[2])
    columns = [
        jnp.dot(flat_rows, matrix, preferred_element_type=jnp.float32).astype(jnp.bfloat16)
        for matrix in weights
    ]
    projected = lax.optimization_barrier(
        jnp.concatenate(columns, axis=1).reshape(piece_rows.shape[0], piece_rows.shape[1], -1)
    )
    key_width = w_query.shape[1]
    value_width = w_value.shape[1]
    heads_here = key_width // KEY
    extent_rows = projected.shape[0]
    seq_count = projected.shape[1]
    bounds_list = [
        0,
        key_width,
        key_width + value_width,
        2 * key_width + value_width,
        3 * key_width + value_width,
        3 * key_width + 2 * value_width,
    ]

    def section_part(position, feature_lanes):
        picked = projected[:, :, bounds_list[position] : bounds_list[position + 1]].astype(
            jnp.float32
        )
        return picked.reshape(extent_rows, seq_count, heads_here, feature_lanes)

    queries = jax.nn.silu(section_part(0, KEY))
    values = section_part(1, VAL)
    shift = decay_shift.reshape(extent_rows, seq_count, heads_here, KEY)
    key_fwd = floor_gap[0].reshape(heads_here, KEY) * jax.nn.sigmoid(-section_part(2, KEY))
    key_bwd = floor_gap[1].reshape(heads_here, KEY) * jax.nn.sigmoid(-section_part(3, KEY))
    decay_fwd = jnp.log1p(-key_fwd) + shift
    decay_bwd = jnp.log1p(-key_bwd) + shift
    fwd_chain = prepare_chain(queries, key_fwd, values, decay_fwd)
    bwd_chain = prepare_chain(queries[::-1], key_bwd[::-1], values[::-1], decay_bwd[::-1])
    identity_pair = (jnp.zeros_like(fwd_chain[6]), jnp.zeros_like(fwd_chain[7]))
    fwd_in = carried_in((fwd_chain[6], fwd_chain[7]), "sp", combine, identity_pair, False)[1]
    bwd_in = carried_in((bwd_chain[6], bwd_chain[7]), "sp", combine, identity_pair, True)[1]
    out_fwd = local_pass(fwd_chain, fwd_in)
    out_bwd = local_pass(bwd_chain, bwd_in)
    combined = out_fwd + out_bwd[::-1]
    head_normed = (
        combined
        * lax.rsqrt(jnp.mean(combined * combined, axis=-1, keepdims=True) + norm_eps)
        * head_gain
    )
    gate_value = jax.nn.silu(projected[:, :, bounds_list[4] : bounds_list[5]].astype(jnp.float32))
    mixed = (head_normed.reshape(extent_rows, seq_count, value_width) * gate_value).astype(
        jnp.bfloat16
    )
    token_rows = lax.all_to_all(mixed, "tp", split_axis=0, concat_axis=2, tiled=True)
    flat_mixed = token_rows.reshape(-1, token_rows.shape[2])
    group_count = lax.axis_size("tp")
    w_columns = lax.all_gather(w_out, "sp", axis=1, tiled=True)
    w_full = lax.all_gather(w_columns, "tp", axis=0, tiled=True)
    accumulated_total = group_sums(flat_mixed, w_full, group_count)
    result = accumulated_total.reshape(token_rows.shape[0], token_rows.shape[1], -1)
    return result.astype(jnp.bfloat16)


def solution(mesh):
    return jax.shard_map(
        shards,
        mesh=mesh,
        in_specs=(
            P(("sp", "tp"), "grp", None),
            P(),
            P("sp", "tp"),
            P("sp", "tp"),
            P("sp", "tp"),
            P("sp", "tp"),
            P("sp", "tp"),
            P(None, "tp"),
            P("sp", "grp", "tp"),
            P(),
            P("tp", "sp"),
        ),
        out_specs=P(("sp", "tp"), "grp", None),
        check_vma=False,
    )
```

profile of v0, /device:TPU:25, one launch (start us, length us, event | category | flops | bytes accessed | tf_op | source)
XLA Modules:
  0.0 473.5 jit_solution(7733809750445567502)
XLA Ops:
  6.5 1.2 fusion.14
  7.8 1.9 fusion.16
  9.7 0.7 all-gather.17.cloned.1.call-update
  10.5 0.7 all-gather.19.cloned.1.call-update
  11.2 0.5 all-gather.21.cloned.1.call-update
  11.8 0.5 all-gather.23.cloned.1.call-update
  12.4 0.5 all-gather.25.cloned.1.call-update
  12.9 0.7 all-gather.27.cloned.1.call-update
  13.7 1.1 reshape.201
  14.8 0.3 reshape.202
  15.1 12.7 %all-gather.15.cloned.1.call-done = bf16[64,4,2048]{2,1,0:T(4,128)(2,1)} async-done(((bf16[16,4,2048]{2,1,0:T(4,128)(2,1)}), bf16[64,4,2048]{2,1,0:T(4,128)(2,1)}) %all-gather.15.cloned.1.call-update) | async-done | bytes 1048592 | tf_op jit(solution)/shard_map/all_gather | solution.py:136
  27.9 1.3 reshape.197
  29.2 43.8 %all-gather.17.cloned.1.call-done = bf16[2048,512]{1,0:T(8,128)(2,1)} async-done(((bf16[512,512]{1,0:T(8,128)(2,1)}), bf16[2048,512]{1,0:T(8,128)(2,1)}) %all-gather.17.cloned.1.call-update) | async-done | bytes 2097168 | tf_op jit(solution)/shard_map/all_gather | solution.py:130
  73.0 3.0 fusion.9
  76.0 43.0 %all-gather.19.cloned.1.call-done = bf16[2048,512]{1,0:T(8,128)(2,1)} async-done(((bf16[512,512]{1,0:T(8,128)(2,1)}), bf16[2048,512]{1,0:T(8,128)(2,1)}) %all-gather.19.cloned.1.call-update) | async-done | bytes 2097168 | tf_op jit(solution)/shard_map/all_gather | solution.py:131
  119.0 3.0 fusion.10
  122.1 42.9 %all-gather.21.cloned.1.call-done = bf16[2048,512]{1,0:T(8,128)(2,1)} async-done(((bf16[512,512]{1,0:T(8,128)(2,1)}), bf16[2048,512]{1,0:T(8,128)(2,1)}) %all-gather.21.cloned.1.call-update) | async-done | bytes 2097168 | tf_op jit(solution)/shard_map/all_gather | solution.py:132
  165.0 3.0 fusion.11
  168.0 42.9 %all-gather.23.cloned.1.call-done = bf16[2048,512]{1,0:T(8,128)(2,1)} async-done(((bf16[512,512]{1,0:T(8,128)(2,1)}), bf16[2048,512]{1,0:T(8,128)(2,1)}) %all-gather.23.cloned.1.call-update) | async-done | bytes 2097168 | tf_op jit(solution)/shard_map/all_gather | solution.py:133
  210.9 3.0 fusion.12
  213.9 42.9 %all-gather.25.cloned.1.call-done = bf16[2048,512]{1,0:T(8,128)(2,1)} async-done(((bf16[512,512]{1,0:T(8,128)(2,1)}), bf16[2048,512]{1,0:T(8,128)(2,1)}) %all-gather.25.cloned.1.call-update) | async-done | bytes 2097168 | tf_op jit(solution)/shard_map/all_gather | solution.py:134
  256.8 3.0 fusion.13
  259.8 2.6 reshape.198
  262.4 1.1 fusion.62
  263.6 0.1 add_divide_fusion.1
  263.7 1.0 div.48
  264.7 1.1 reshape.209
  265.8 0.1 reshape.216
  265.9 0.1 add_divide_fusion
  266.1 0.2 reshape.215
  266.2 1.2 log-plus-one_add_fusion
  267.8 3.0 fusion.36
  270.8 1.5 fusion.26
  272.4 2.8 fusion.5
  275.2 0.2 all-gather.31.cloned.1.call-start
  275.5 1.0 reshape.214
  276.5 2.5 fusion.35
  278.9 2.0 fusion.4
  281.0 21.8 %all-gather.27.cloned.1.call-done = bf16[512,2048]{1,0:T(8,128)(2,1)} async-done(((bf16[512,512]{1,0:T(8,128)(2,1)}), bf16[512,2048]{1,0:T(8,128)(2,1)}) %all-gather.27.cloned.1.call-update) | async-done | bytes 2097168 | tf_op jit(solution)/shard_map/all_gather | solution.py:192
  302.9 10.5 %all-gather = bf16[4,1,4,4,128]{4,3,2,1,0:T(4,128)(2,1)S(1)} all-gather(bf16[1,1,4,4,128]{4,3,2,1,0:T(4,128)(2,1)S(1)} %slice.123), channel_id=2, replica_groups=mesh['grp'=2,'sp'=4,'tp'=4] {'sp'}, dimensions={0}, use_global_device_ids=true | all-gather | bytes 20480 | tf_op jit(solution)/shard_map/all_gather | solution.py:18
  313.4 10.9 %all-gather.2 = bf16[4,1,4,4,128]{4,3,2,1,0:T(4,128)(2,1)S(1)} all-gather(bf16[1,1,4,4,128]{4,3,2,1,0:T(4,128)(2,1)S(1)} %slice.122), channel_id=4, replica_groups=mesh['grp'=2,'sp'=4,'tp'=4] {'sp'}, dimensions={0}, use_global_device_ids=true | all-gather | bytes 20480 | tf_op jit(solution)/shard_map/all_gather | solution.py:18
  324.2 2.4 convolution_select_fusion.1
  326.7 1.2 fusion.56
  327.9 1.2 convolution_select_fusion
  329.1 0.6 fusion.52
  329.7 19.4 %all-gather.33.cloned.1.call-done = bf16[16,4,128,128]{3,2,1,0:T(8,128)(2,1)} async-done(((bf16[4,4,128,128]{3,2,1,0:T(8,128)(2,1)}), bf16[16,4,128,128]{3,2,1,0:T(8,128)(2,1)}) %all-gather.33.cloned.1.call-update) | async-done | bytes 2097168 | tf_op jit(solution)/shard_map/all_gather | solution.py:18
  349.2 1.1 fusion.6
  350.4 44.8 %all-gather.31.cloned.1.call-done = bf16[16,4,128,128]{3,2,1,0:T(8,128)(2,1)} async-done(((bf16[4,4,128,128]{3,2,1,0:T(8,128)(2,1)}), bf16[16,4,128,128]{3,2,1,0:T(8,128)(2,1)}) %all-gather.31.cloned.1.call-update) | async-done | bytes 2097168 | tf_op jit(solution)/shard_map/all_gather | solution.py:18
  395.4 4.9 %while.26 = (s32[]{:T(128)}, f32[4,4,128,128]{3,2,1,0:T(8,128)S(1)}, s32[]{:T(128)}, bf16[4,4,4,128]{3,2,1,0:T(4,128)(2,1)S(1)}, bf16[4,4,4,128,128]{4,3,2,1,0:T(8,128)(2,1)}, /*index=5*/s32[]{:T(128)}, s32[]{:T(128)}, s32[]{:T(128)}) while((s32[]{:T(128)}, f32[4,4,128,128]{3,2,1,0:T(8,128)S(1)}, s32[]{:T(128)}, ...), condition=%wide.region_3.4_spmd, body=%wide.region_2.3_spmd.sunk | while | flops 788485 | bytes 2642047 | solution.py:33
  395.4 1.6 convert_add_fusion.4
  397.1 1.5 convert_add_fusion.4
  398.7 1.5 convert_add_fusion.4
  400.3 1.2 multiply_reduce_fusion
  401.6 0.2 fusion.50
  401.8 0.2 copy.53
  402.0 9.5 %all_to_all.15 = bf16[64,4,512]{2,1,0:T(4,128)(2,1)S(1)} all-to-all(bf16[64,4,512]{2,1,0:T(4,128)(2,1)S(1)} %copy.53), channel_id=1, replica_groups=mesh['grp'=2,'sp'=4,'tp'=4] {'tp'}, dimensions={0} | all-to-all | bytes 524288 | tf_op jit(solution)/shard_map/all_to_all | solution.py:189
  411.5 0.2 copy.54
  411.8 45.6 %all-gather.29.cloned.1.call-done = bf16[2048,2048]{1,0:T(8,128)(2,1)} async-done(((bf16[512,2048]{1,0:T(8,128)(2,1)}), bf16[2048,2048]{1,0:T(8,128)(2,1)}) %all-gather.29.cloned.1.call-update) | async-done | bytes 8388624 | tf_op jit(solution)/shard_map/all_gather | solution.py:193
  457.4 2.1 convolution_convert_fusion.3
  459.5 2.1 convolution_convert_fusion.2
  461.5 2.1 convolution_convert_fusion.1
  463.6 2.1 convolution_convert_fusion
  465.7 0.1 add_convert_fusion
  465.8 0.8 convert_element_type.171
  (53 shorter events, 1.1 us)
Async XLA Ops:
  6.5 7.2 %copy-start.3 = (f32[64,4,512]{2,1,0:T(4,128)S(1)}, f32[64,4,512]{2,1,0:T(4,128)}, u32[]{:S(2)}) copy-start(f32[64,4,512]{2,1,0:T(4,128)} %param.23) | copy-start | bytes 1572868
  6.5 21.3 %all-gather.15.cloned.1.call-start = ((), (), s32[]{:S(2)}) async-start(), calls=%async_computation.1 | async-start | bytes 1310720 | tf_op jit(solution)/shard_map/all_gather | solution.py:136
  9.7 63.3 %all-gather.17.cloned.1.call-start = ((), (), s32[]{:S(2)}) async-start(), calls=%async_computation.2 | async-start | bytes 2621440 | tf_op jit(solution)/shard_map/all_gather | solution.py:130
  10.4 108.6 %all-gather.19.cloned.1.call-start = ((), (), s32[]{:S(2)}) async-start(), calls=%async_computation.3 | async-start | bytes 2621440 | tf_op jit(solution)/shard_map/all_gather | solution.py:131
  11.1 4.0 copy-start.7
  11.2 153.8 %all-gather.21.cloned.1.call-start = ((), (), s32[]{:S(2)}) async-start(), calls=%async_computation.4 | async-start | bytes 2621440 | tf_op jit(solution)/shard_map/all_gather | solution.py:132
  11.7 199.1 %all-gather.23.cloned.1.call-start = ((), (), s32[]{:S(2)}) async-start(), calls=%async_computation.5 | async-start | bytes 2621440 | tf_op jit(solution)/shard_map/all_gather | solution.py:133
  12.3 244.5 %all-gather.25.cloned.1.call-start = ((), (), s32[]{:S(2)}) async-start(), calls=%async_computation.6 | async-start | bytes 2621440 | tf_op jit(solution)/shard_map/all_gather | solution.py:134
  12.9 290.0 %all-gather.27.cloned.1.call-start = ((), (), s32[]{:S(2)}) async-start(), calls=%async_computation.7 | async-start | bytes 2621440 | tf_op jit(solution)/shard_map/all_gather | solution.py:192
  13.6 335.5 %all-gather.33.cloned.1.call-start = ((), (), s32[]{:S(2)}) async-start(), calls=%async_computation.10 | async-start | bytes 2621440 | tf_op jit(solution)/shard_map/all_gather | solution.py:18
  267.7 3.2 copy-start.2
  275.2 120.0 %all-gather.31.cloned.1.call-start = ((), (), s32[]{:S(2)}) async-start(), calls=%async_computation.9 | async-start | bytes 2621440 | tf_op jit(solution)/shard_map/all_gather | solution.py:18
  281.0 176.4 %all-gather.29.cloned.1.call-start = ((), (), s32[]{:S(2)}) async-start(), calls=%async_computation.8 | async-start | bytes 10485760 | tf_op jit(solution)/shard_map/all_gather | solution.py:193
  302.9 25.0 %copy-start = (f32[64,4,4,128]{3,2,1,0:T(4,128)S(1)}, f32[64,4,4,128]{3,2,1,0:T(4,128)}, u32[]{:S(2)}) copy-start(f32[64,4,4,128]{3,2,1,0:T(4,128)} %get-tuple-element.169) | copy-start | bytes 1572868
  302.9 25.0 %copy-start.1 = (f32[64,4,4,128]{3,2,1,0:T(4,128)S(1)}, f32[64,4,4,128]{3,2,1,0:T(4,128)}, u32[]{:S(2)}) copy-start(f32[64,4,4,128]{3,2,1,0:T(4,128)} %get-tuple-element.170) | copy-start | bytes 1572868
  395.4 4.9 %copy-start.4 = (f32[4,4,128,64]{2,3,1,0:T(8,128)S(1)}, f32[4,4,128,64]{2,3,1,0:T(8,128)}, u32[]{:S(2)}) copy-start(f32[4,4,128,64]{2,3,1,0:T(8,128)} %fusion.56) | copy-start | bytes 1572868
  395.4 4.9 %copy-start.5 = (f32[64,4,4,128]{3,2,1,0:T(4,128)S(1)}, f32[64,4,4,128]{3,2,1,0:T(4,128)}, u32[]{:S(2)}) copy-start(f32[64,4,4,128]{3,2,1,0:T(4,128)} %get-tuple-element.155) | copy-start | bytes 1572868
  400.3 1.3 copy-start.6
  400.3 1.3 copy-start.8
Sparse Core Ops, SparseCore 0:
  9.8 18.0 all-gather.14
  29.4 43.4 all-gather.16
  74.5 44.4 all-gather.18
  120.5 44.4 all-gather.20
  166.4 44.4 all-gather.22
  212.3 44.4 all-gather.24
  258.4 44.4 all-gather.26
  304.4 44.6 all-gather.32
  350.7 44.5 all-gather.30
  396.7 60.6 all-gather.28
where the time goes:
time: 474 us; the launch traced here: 473 us
  waiting for transfers between devices  364 us (77%)
  matrix products  36.1 us (8%)
  blocking collectives  30.8 us (6%)
  other arithmetic  18.1 us (4%)
  between operations  13.9 us (3%)
  local copies, waits for them, and re-layouts  10.4 us (2%)
    all_gather x2, waiting for transfers between devices, carried_in(): lax.all_gather(a.astype(kind), axis)  64.2 us
    all_gather x1, waiting for transfers between devices, shards(): w_full = lax.all_gather(w_columns, 'tp', axis=0, tiled=True)  45.6 us
    all_gather x1, waiting for transfers between devices, shards(): lax.all_gather(w_query, 'sp', axis=0, tiled=True)  43.8 us
    all_gather x1, waiting for transfers between devices, shards(): lax.all_gather(w_value, 'sp', axis=0, tiled=True)  43 us
    all_gather x1, waiting for transfers between devices, shards(): lax.all_gather(w_out_gate, 'sp', axis=0, tiled=True)  42.9 us
    all_gather x1, waiting for transfers between devices, shards(): lax.all_gather(w_bwd_gate, 'sp', axis=0, tiled=True)  42.9 us
    all_gather x1, waiting for transfers between devices, shards(): lax.all_gather(w_fwd_gate, 'sp', axis=0, tiled=True)  42.9 us
    all_gather x1, waiting for transfers between devices, shards(): w_columns = lax.all_gather(w_out, 'sp', axis=1, tiled=True)  21.8 us
  transfers between devices with their start and end apart: 10, of which 10 were waited for; matrix products, arithmetic and copies ran while one was open for 11% of the time, Pallas kernels for 0%

commit v1 on v0

--- a/solution.py
+++ b/solution.py
@@ -8,6 +8,17 @@
 BLOCK = 64
 norm_eps = 1e-06
 highest = lax.Precision.HIGHEST
+
+
+def pass_along(x, mesh_axis, along):
+    devices = lax.axis_size(mesh_axis)
+    hops = [(i, (i + 1) % devices) for i in range(devices)]
+    blocks = [x]
+    for reach in range(1, devices):
+        blocks = [lax.ppermute(blocks[0], mesh_axis, hops), *blocks]
+    result = jnp.concatenate(blocks, axis=along)
+    places = (lax.axis_index(mesh_axis) + 1) * blocks[-1].shape[along]
+    return jnp.roll(result, places, axis=along)
 
 
 def carried_in(x, axis, join, neutral, backward):
@@ -190,7 +201,7 @@
     flat_mixed = token_rows.reshape(-1, token_rows.shape[2])
     group_count = lax.axis_size("tp")
     w_columns = lax.all_gather(w_out, "sp", axis=1, tiled=True)
-    w_full = lax.all_gather(w_columns, "tp", axis=0, tiled=True)
+    w_full = pass_along(w_columns, "tp", 0)
     accumulated_total = group_sums(flat_mixed, w_full, group_count)
     result = accumulated_total.reshape(token_rows.shape[0], token_rows.shape[1], -1)
     return result.astype(jnp.bfloat16)

time: 474 us -> 433 us (0.914)
  waiting for transfers between devices: 364 us -> 311 us
  starting transfers between devices: 0.54 us -> 13.8 us
  local copies, waits for them, and re-layouts: 10.4 us -> 22.7 us
  blocking collectives: 30.8 us -> 21.7 us
  matrix products: 36.1 us -> 30.1 us
    all_gather x1 -> x0, waiting for transfers between devices: 45.6 us -> none  [shards(): w_full = lax.all_gather(w_columns, 'tp', axis=0, tiled=True)]
    all_gather x2, waiting for transfers between devices: 64.2 us -> 27.3 us  [carried_in(): lax.all_gather(a.astype(kind), axis)]
    ppermute x0 -> x3, waiting for transfers between devices: none -> 14 us  [pass_along(): blocks = [lax.ppermute(blocks[0], mesh_axis, hops), *blocks]]
    unnamed x19 -> x34, local copies, waits for them, and re-layouts: 0.09 us -> 9.77 us
    ppermute x0 -> x3, starting transfers between devices: none -> 9.57 us  [pass_along(): blocks = [lax.ppermute(blocks[0], mesh_axis, hops), *blocks]]
    all_to_all x1 -> x0, blocking collectives: 9.49 us -> none  [shards(): lax.all_to_all(mixed, 'tp', split_axis=0, concat_axis=2, tiled=True)]
    all_gather x1, waiting for transfers between devices: 21.8 us -> 30.3 us  [shards(): w_columns = lax.all_gather(w_out, 'sp', axis=1, tiled=True)]
    dot_general x4, matrix products: 8.28 us -> 1.95 us  [group_sums(): jnp.dot(flat_mixed[:, first_column:first_column + group_width], weight_li...]
  transfers between devices with their start and end apart: 10 -> 13, of which waited for: 10 -> 11; matrix products, arithmetic and copies ran while one was open for 11% -> 13% of each run, Pallas kernels for 0% -> 0%
where the time goes in v1:
time: 433 us; the launch traced here: 432 us
  waiting for transfers between devices  311 us (72%)
  matrix products  30.1 us (7%)
  local copies, waits for them, and re-layouts  22.7 us (5%)
  blocking collectives  21.7 us (5%)
  other arithmetic  18.5 us (4%)
  starting transfers between devices  13.8 us (3%)
  between operations  13.7 us (3%)
    all_gather x1, waiting for transfers between devices, shards(): lax.all_gather(w_value, 'sp', axis=0, tiled=True)  43.8 us
    all_gather x1, waiting for transfers between devices, shards(): lax.all_gather(w_query, 'sp', axis=0, tiled=True)  43.8 us
    all_gather x1, waiting for transfers between devices, shards(): lax.all_gather(w_fwd_gate, 'sp', axis=0, tiled=True)  43.6 us
    all_gather x1, waiting for transfers between devices, shards(): lax.all_gather(w_out_gate, 'sp', axis=0, tiled=True)  43.6 us
    all_gather x1, waiting for transfers between devices, shards(): lax.all_gather(w_bwd_gate, 'sp', axis=0, tiled=True)  43.6 us
    all_gather x1, waiting for transfers between devices, shards(): w_columns = lax.all_gather(w_out, 'sp', axis=1, tiled=True)  30.3 us
    all_gather x2, waiting for transfers between devices, carried_in(): lax.all_gather(a.astype(kind), axis)  27.3 us
    all_gather x2, blocking collectives, carried_in(): lax.all_gather(a.astype(kind), axis)  21.7 us
  transfers between devices with their start and end apart: 13, of which 11 were waited for; matrix products, arithmetic and copies ran while one was open for 13% of the time, Pallas kernels for 0%

profile of v1, /device:TPU:25, one launch (start us, length us, event | category | flops | bytes accessed | tf_op | source)
XLA Modules:
  0.0 432.0 jit_solution(5856848597347600547)
XLA Ops:
  6.5 1.2 fusion.14
  7.8 1.9 fusion.16
  9.7 0.7 all-gather.16.cloned.1.call-update
  10.5 0.7 all-gather.18.cloned.1.call-update
  11.2 0.5 all-gather.20.cloned.1.call-update
  11.8 0.5 all-gather.22.cloned.1.call-update
  12.4 0.5 all-gather.24.cloned.1.call-update
  12.9 0.7 all-gather.26.cloned.1.call-update
  14.0 1.1 reshape.201
  15.1 12.8 %all-gather.14.cloned.1.call-done = bf16[64,4,2048]{2,1,0:T(4,128)(2,1)} async-done(((bf16[16,4,2048]{2,1,0:T(4,128)(2,1)}), bf16[64,4,2048]{2,1,0:T(4,128)(2,1)}) %all-gather.14.cloned.1.call-update) | async-done | bytes 1048592 | tf_op jit(solution)/shard_map/all_gather | solution.py:147
  27.9 1.3 reshape.197
  29.2 43.8 %all-gather.16.cloned.1.call-done = bf16[2048,512]{1,0:T(8,128)(2,1)} async-done(((bf16[512,512]{1,0:T(8,128)(2,1)}), bf16[2048,512]{1,0:T(8,128)(2,1)}) %all-gather.16.cloned.1.call-update) | async-done | bytes 2097168 | tf_op jit(solution)/shard_map/all_gather | solution.py:141
  73.0 2.3 fusion.9
  75.3 43.8 %all-gather.18.cloned.1.call-done = bf16[2048,512]{1,0:T(8,128)(2,1)} async-done(((bf16[512,512]{1,0:T(8,128)(2,1)}), bf16[2048,512]{1,0:T(8,128)(2,1)}) %all-gather.18.cloned.1.call-update) | async-done | bytes 2097168 | tf_op jit(solution)/shard_map/all_gather | solution.py:142
  119.0 2.3 fusion.10
  121.3 43.6 %all-gather.20.cloned.1.call-done = bf16[2048,512]{1,0:T(8,128)(2,1)} async-done(((bf16[512,512]{1,0:T(8,128)(2,1)}), bf16[2048,512]{1,0:T(8,128)(2,1)}) %all-gather.20.cloned.1.call-update) | async-done | bytes 2097168 | tf_op jit(solution)/shard_map/all_gather | solution.py:143
  165.0 2.3 fusion.11
  167.3 43.6 %all-gather.22.cloned.1.call-done = bf16[2048,512]{1,0:T(8,128)(2,1)} async-done(((bf16[512,512]{1,0:T(8,128)(2,1)}), bf16[2048,512]{1,0:T(8,128)(2,1)}) %all-gather.22.cloned.1.call-update) | async-done | bytes 2097168 | tf_op jit(solution)/shard_map/all_gather | solution.py:144
  210.9 2.3 fusion.12
  213.2 43.6 %all-gather.24.cloned.1.call-done = bf16[2048,512]{1,0:T(8,128)(2,1)} async-done(((bf16[512,512]{1,0:T(8,128)(2,1)}), bf16[2048,512]{1,0:T(8,128)(2,1)}) %all-gather.24.cloned.1.call-update) | async-done | bytes 2097168 | tf_op jit(solution)/shard_map/all_gather | solution.py:145
  256.8 2.3 fusion.13
  259.4 1.2 fusion.66
  261.5 1.1 reshape.209
  262.8 1.0 div.48
  264.2 3.1 fusion.36
  267.3 0.8 copy-done.1
  268.1 1.6 fusion.26
  269.6 2.8 fusion.5
  272.6 30.3 %all-gather.26.cloned.1.call-done = bf16[512,2048]{1,0:T(8,128)(2,1)} async-done(((bf16[512,512]{1,0:T(8,128)(2,1)}), bf16[512,2048]{1,0:T(8,128)(2,1)}) %all-gather.26.cloned.1.call-update) | async-done | bytes 2097168 | tf_op jit(solution)/shard_map/all_gather | solution.py:203
  302.9 1.3 collective-permute-start
  304.2 1.0 reshape.214
  305.2 0.7 exponential_multiply_fusion.1
  305.9 0.7 slice_bitcast_fusion.3
  306.6 2.9 fusion.35
  309.5 2.0 fusion.4
  311.6 0.8 slice.110
  312.4 0.7 slice.111
  313.1 10.9 %all-gather.2 = bf16[4,1,4,4,128]{4,3,2,1,0:T(4,128)(2,1)S(1)} all-gather(bf16[1,1,4,4,128]{4,3,2,1,0:T(4,128)(2,1)S(1)} %slice.110), channel_id=4, replica_groups=mesh['grp'=2,'sp'=4,'tp'=4] {'sp'}, dimensions={0}, use_global_device_ids=true | all-gather | bytes 20480 | tf_op jit(solution)/shard_map/all_gather | solution.py:29
  323.9 10.9 %all-gather = bf16[4,1,4,4,128]{4,3,2,1,0:T(4,128)(2,1)S(1)} all-gather(bf16[1,1,4,4,128]{4,3,2,1,0:T(4,128)(2,1)S(1)} %slice.111), channel_id=2, replica_groups=mesh['grp'=2,'sp'=4,'tp'=4] {'sp'}, dimensions={0}, use_global_device_ids=true | all-gather | bytes 20480 | tf_op jit(solution)/shard_map/all_gather | solution.py:29
  334.8 2.2 convolution_select_fusion
  337.0 1.4 fusion.52
  338.5 1.2 convolution_select_fusion.1
  339.7 5.6 %collective-permute-start.1 = (bf16[512,2048]{1,0:T(8,128)(2,1)S(1)}, bf16[512,2048]{1,0:T(8,128)(2,1)}, u32[]{:S(2)}, u32[]{:S(2)}) collective-permute-start(bf16[512,2048]{1,0:T(8,128)(2,1)S(1)} %collective-permute-done), channel_id=1, source_target_pairs={{0,1},{1,2},{2,3},{3,0},{4,5},{5,6},{6,7},{7,4},{8,9},{9,10},{10,1... | collective-permute-start | bytes 6291464 | tf_op jit(solution)/shard_map/ppermute | solution.py:18
  345.3 1.2 fusion.56
  346.5 2.7 all-gather.30.cloned.1.call-done
  349.4 3.1 fusion.6
  352.5 1.9 rev.19
  354.4 13.9 %collective-permute-done.1 = bf16[512,2048]{1,0:T(8,128)(2,1)} collective-permute-done((bf16[512,2048]{1,0:T(8,128)(2,1)S(1)}, bf16[512,2048]{1,0:T(8,128)(2,1)}, u32[]{:S(2)}, u32[]{:S(2)}) %collective-permute-start.1) | collective-permute-done | bytes 2097184 | tf_op jit(solution)/shard_map/ppermute | solution.py:18
  368.3 2.6 collective-permute-start.2
  370.9 24.6 %all-gather.28.cloned.1.call-done = bf16[16,4,128,128]{3,2,1,0:T(8,128)(2,1)} async-done(((bf16[4,4,128,128]{3,2,1,0:T(8,128)(2,1)}), bf16[16,4,128,128]{3,2,1,0:T(8,128)(2,1)}) %all-gather.28.cloned.1.call-update) | async-done | bytes 2097168 | tf_op jit(solution)/shard_map/all_gather | solution.py:29
  395.6 4.8 %while.26 = (s32[]{:T(128)}, f32[4,4,128,128]{3,2,1,0:T(8,128)S(1)}, s32[]{:T(128)}, bf16[4,4,4,128]{3,2,1,0:T(4,128)(2,1)S(1)}, bf16[4,4,4,128,128]{4,3,2,1,0:T(8,128)(2,1)}, /*index=5*/s32[]{:T(128)}, s32[]{:T(128)}, s32[]{:T(128)}) while((s32[]{:T(128)}, f32[4,4,128,128]{3,2,1,0:T(8,128)S(1)}, s32[]{:T(128)}, ...), condition=%wide.region_3.4_spmd, body=%wide.region_2.3_spmd.sunk | while | flops 788485 | bytes 2642055 | solution.py:44
  395.7 1.5 convert_add_fusion.4
  397.3 1.5 convert_add_fusion.4
  398.9 1.5 convert_add_fusion.4
  400.4 2.6 multiply_reduce_fusion
  403.3 0.9 copy.53
  404.2 3.9 all-to-all-start
  408.1 5.0 %all-to-all-done = bf16[64,4,512]{2,1,0:T(4,128)(2,1)S(1)} async-done(((bf16[64,4,512]{2,1,0:T(4,128)(2,1)}), bf16[64,4,512]{2,1,0:T(4,128)(2,1)S(1)}, u32[]{:S(2)}, u32[]{:S(2)}) %all-to-all-start) | async-done | bytes 262176 | tf_op jit(solution)/shard_map/all_to_all | solution.py:200
  413.4 1.7 constant_dynamic-update-slice_fusion.7
  415.1 1.7 constant_dynamic-update-slice_fusion.6
  417.0 1.4 copy-done
  418.7 1.7 constant_dynamic-update-slice_fusion.3
  420.4 1.7 constant_dynamic-update-slice_fusion.2
  424.7 0.8 convert_element_type.171
  (73 shorter events, 6.0 us)
Async XLA Ops:
  6.5 7.2 %copy-start.4 = (f32[64,4,512]{2,1,0:T(4,128)S(1)}, f32[64,4,512]{2,1,0:T(4,128)}, u32[]{:S(2)}) copy-start(f32[64,4,512]{2,1,0:T(4,128)} %param.23) | copy-start | bytes 1572868
  6.5 21.3 %all-gather.14.cloned.1.call-start = ((), (), s32[]{:S(2)}) async-start(), calls=%async_computation.1 | async-start | bytes 1310720 | tf_op jit(solution)/shard_map/all_gather | solution.py:147
  9.7 63.3 %all-gather.16.cloned.1.call-start = ((), (), s32[]{:S(2)}) async-start(), calls=%async_computation.2 | async-start | bytes 2621440 | tf_op jit(solution)/shard_map/all_gather | solution.py:141
  10.4 108.6 %all-gather.18.cloned.1.call-start = ((), (), s32[]{:S(2)}) async-start(), calls=%async_computation.3 | async-start | bytes 2621440 | tf_op jit(solution)/shard_map/all_gather | solution.py:142
  11.1 4.0 copy-start.11
  11.2 153.8 %all-gather.20.cloned.1.call-start = ((), (), s32[]{:S(2)}) async-start(), calls=%async_computation.4 | async-start | bytes 2621440 | tf_op jit(solution)/shard_map/all_gather | solution.py:143
  11.7 199.1 %all-gather.22.cloned.1.call-start = ((), (), s32[]{:S(2)}) async-start(), calls=%async_computation.5 | async-start | bytes 2621440 | tf_op jit(solution)/shard_map/all_gather | solution.py:144
  12.3 244.5 %all-gather.24.cloned.1.call-start = ((), (), s32[]{:S(2)}) async-start(), calls=%async_computation.6 | async-start | bytes 2621440 | tf_op jit(solution)/shard_map/all_gather | solution.py:145
  12.9 290.0 %all-gather.26.cloned.1.call-start = ((), (), s32[]{:S(2)}) async-start(), calls=%async_computation.7 | async-start | bytes 2621440 | tf_op jit(solution)/shard_map/all_gather | solution.py:203
  13.6 335.6 %all-gather.30.cloned.1.call-start = ((), (), s32[]{:S(2)}) async-start(), calls=%async_computation.9 | async-start | bytes 2621440 | tf_op jit(solution)/shard_map/all_gather | solution.py:29
  261.0 1.6 copy-start.8
  261.4 2.3 copy-start.9
  262.7 1.4 copy-start.7
  264.1 5.5 %copy-start.2 = (f32[1,64,4,4,128]{4,3,2,1,0:T(4,128)}, f32[1,64,4,4,128]{4,3,2,1,0:T(4,128)S(1)}, u32[]{:S(2)}) copy-start(f32[1,64,4,4,128]{4,3,2,1,0:T(4,128)S(1)} %fusion.28) | copy-start | bytes 1572868
  267.3 0.8 copy-start.1
  272.5 123.0 %all-gather.28.cloned.1.call-start = ((), (), s32[]{:S(2)}) async-start(), calls=%async_computation.8 | async-start | bytes 2621440 | tf_op jit(solution)/shard_map/all_gather | solution.py:29
  302.9 36.8 %collective-permute-start = (bf16[512,2048]{1,0:T(8,128)(2,1)}, bf16[512,2048]{1,0:T(8,128)(2,1)S(1)}, u32[]{:S(2)}, u32[]{:S(2)}) collective-permute-start(bf16[512,2048]{1,0:T(8,128)(2,1)} %all-gather.26.cloned.1.call-done), channel_id=1, source_target_pairs={{0,1},{1,2},{2,3},{3,0},{4,5},{5,6},{6,7},{7,4},{8,9},{9,10},{10,1... | collective-permute-start | bytes 6291464 | tf_op jit(solution)/shard_map/ppermute | solution.py:18
  306.6 28.2 %copy-start.3 = (f32[64,4,4,128]{3,2,1,0:T(4,128)S(1)}, f32[64,4,4,128]{3,2,1,0:T(4,128)}, u32[]{:S(2)}) copy-start(f32[64,4,4,128]{3,2,1,0:T(4,128)} %get-tuple-element.169) | copy-start | bytes 1572868
  311.5 26.9 %copy-start.5 = (f32[64,4,4,128]{3,2,1,0:T(4,128)S(1)}, f32[64,4,4,128]{3,2,1,0:T(4,128)}, u32[]{:S(2)}) copy-start(f32[64,4,4,128]{3,2,1,0:T(4,128)} %get-tuple-element.165) | copy-start | bytes 1572868
  311.5 26.9 %copy-start.6 = (f32[64,4,4,128]{3,2,1,0:T(4,128)S(1)}, f32[64,4,4,128]{3,2,1,0:T(4,128)}, u32[]{:S(2)}) copy-start(f32[64,4,4,128]{3,2,1,0:T(4,128)} %get-tuple-element.172) | copy-start | bytes 1572868
  339.7 28.6 %collective-permute-start.1 = (bf16[512,2048]{1,0:T(8,128)(2,1)S(1)}, bf16[512,2048]{1,0:T(8,128)(2,1)}, u32[]{:S(2)}, u32[]{:S(2)}) collective-permute-start(bf16[512,2048]{1,0:T(8,128)(2,1)S(1)} %collective-permute-done), channel_id=1, source_target_pairs={{0,1},{1,2},{2,3},{3,0},{4,5},{5,6},{6,7},{7,4},{8,9},{9,10},{10,1... | collective-permute-start | bytes 6291464 | tf_op jit(solution)/shard_map/ppermute | solution.py:18
  368.3 45.1 %collective-permute-start.2 = (bf16[512,2048]{1,0:T(8,128)(2,1)}, bf16[512,2048]{1,0:T(8,128)(2,1)}, u32[]{:S(2)}, u32[]{:S(2)}) collective-permute-start(bf16[512,2048]{1,0:T(8,128)(2,1)} %collective-permute-done.1), channel_id=1, source_target_pairs={{0,1},{1,2},{2,3},{3,0},{4,5},{5,6},{6,7},{7,4},{8,9},{9,10},{10,1... | collective-permute-start | bytes 6291464 | tf_op jit(solution)/shard_map/ppermute | solution.py:18
  400.4 2.6 copy-start.10
  400.4 2.6 copy-start.12
  404.2 8.9 %all-to-all-start = ((bf16[64,4,512]{2,1,0:T(4,128)(2,1)}), bf16[64,4,512]{2,1,0:T(4,128)(2,1)S(1)}, u32[]{:S(2)}, u32[]{:S(2)}) async-start(bf16[64,4,512]{2,1,0:T(4,128)(2,1)} %copy.53), calls=%async_computation | async-start | bytes 524288 | tf_op jit(solution)/shard_map/all_to_all | solution.py:200
  416.9 1.6 copy-start
Sparse Core Ops, SparseCore 0:
  9.8 18.0 all-gather.13
  29.4 43.4 all-gather.15
  74.5 44.4 all-gather.17
  120.5 44.4 all-gather.19
  166.4 44.4 all-gather.21
  212.3 44.4 all-gather.23
  258.4 44.4 all-gather.25
  304.4 44.7 all-gather.29
  350.8 44.6 all-gather.27
